TPU v7x, 512 devices: a whole 4x8x8 slice. The times are simulated.
512 devices in a mesh: sp: 64 (over z, y), tp: 8 (over x, core).
Axes of the slice: x: 4, y: 8, z: 8, core: 2. Of those that a mesh axis runs over, the one named last changes fastest.
Arguments:
- queries: bfloat16 [32768, 2048], P('sp', 'tp'), may hold values from -14 to 14
- key_states: bfloat16 [32768, 512], P('sp', 'tp'), may hold values from -14 to 14
- value_states: bfloat16 [32768, 512], P('sp', 'tp'), may hold values from -6 to 6
- sink_logits: float32 [32], P('tp'), may hold values from 0 to 5
- out_weight: bfloat16 [2048, 2048], P('tp'), may hold values from -0.125 to 0.125
- residual: bfloat16 [32768, 2048], P(('sp', 'tp')), may hold values from -6 to 6
- gain_attn: float32 [2048], replicated, may hold values from 0.1 to 1.9
- gain_before: float32 [2048], replicated, may hold values from 0.1 to 1.9
- gain_after: float32 [2048], replicated, may hold values from 0.1 to 1.9
- gate_weight: bfloat16 [2048, 5632], P('sp', 'tp'), may hold values from -0.125 to 0.125
- value_weight: bfloat16 [2048, 5632], P('sp', 'tp'), may hold values from -0.125 to 0.125
- gate_taps: float32 [3, 5632], P(None, 'tp'), may hold values from -3 to 3
- value_taps: float32 [3, 5632], P(None, 'tp'), may hold values from -3 to 3
- down_weight: bfloat16 [5632, 2048], P('tp', 'sp'), may hold values from -0.078125 to 0.078125
Outputs:
- layer_out: bfloat16 [32768, 2048], P(('sp', 'tp'))
All inputs are finite; a program needn't handle non-finite values.
Results may differ from a plain program's by a relative error of at most 0.018.
Values may be sent and summed in bfloat16 or wider, within the bound.
A program may use at most 64 MiB of HBM per device.

v0:
```python
import jax
import jax.numpy as jnp
from jax import lax
from jax.sharding import PartitionSpec as P

HD = 64
WINDOW = 128
NEG_FILL = -1e30


def passed_along(block, axis, distance):
    devices = range(lax.axis_size(axis))
    route = [(i - distance, i) for i in devices if i - distance in devices]
    return lax.ppermute(block, axis, route)


def in_blocks(shard, dim, peers):
    before, after = (shard.shape[:dim], shard.shape[dim + 1 :])
    return jnp.moveaxis(shard.reshape(*before, peers, -1, *after), dim, 0)


def sum_at_owner(shard, axis, dim):
    peers = lax.axis_size(axis)
    pieces = lax.all_to_all(in_blocks(shard, dim, peers), axis, 0, 0, tiled=True)
    return jnp.sum(pieces.astype(jnp.float32), axis=0)


def in_order(pieces, dim):
    pieces = jnp.moveaxis(pieces, 0, dim)
    lengths = pieces.shape
    return pieces.reshape(*lengths[:dim], lengths[dim] * lengths[dim + 1], *lengths[dim + 2 :])


def sent_to_all(shard, axis):
    copies = jnp.broadcast_to(shard, (lax.axis_size(axis), *shard.shape))
    return lax.all_to_all(copies, axis, split_axis=0, concat_axis=0, tiled=True)


def gather_directly(shard, axis, dim):
    return in_order(sent_to_all(shard, axis), dim)


def in_one_piece(arrays, axis, dim, along):
    widths = [a.shape[along] for a in arrays]
    both = jnp.concatenate(arrays, axis=along)
    filled = lax.all_gather(both, axis, axis=dim, tiled=True)
    return tuple(jnp.split(filled, [sum(widths[:k]) for k in range(1, len(widths))], axis=along))


def rms_scale(matrix):
    return matrix * lax.rsqrt(jnp.mean(matrix * matrix, axis=-1, keepdims=True) + 1e-06)


def attention_local(queries, key_states, value_states, sink_logits):
    length = queries.shape[0]
    blocks = length // WINDOW
    kv_local = key_states.shape[1] // HD
    grouping = queries.shape[1] // key_states.shape[1]
    earlier_keys, earlier_values = passed_along(
        (key_states[length - WINDOW :], value_states[length - WINDOW :]), "sp", 1
    )
    keys_ext = jnp.concatenate([earlier_keys, key_states], axis=0).reshape(
        blocks + 1, WINDOW, kv_local, HD
    )
    values_ext = jnp.concatenate([earlier_values, value_states], axis=0).reshape(
        blocks + 1, WINDOW, kv_local, HD
    )
    key_blocks = jnp.concatenate([keys_ext[:-1], keys_ext[1:]], axis=1)
    value_blocks = jnp.concatenate([values_ext[:-1], values_ext[1:]], axis=1)
    query_blocks = queries.reshape(blocks, WINDOW, kv_local, grouping, HD)
    offset = lax.axis_index("sp") * length
    qpos = (offset + jnp.arange(length, dtype=jnp.int32)).reshape(blocks, WINDOW)
    kpos = jnp.concatenate([qpos - WINDOW, qpos], axis=1)
    visible = (
        (kpos[:, None, :] <= qpos[:, :, None])
        & (qpos[:, :, None] - kpos[:, None, :] < WINDOW)
        & (kpos[:, None, :] >= 0)
    )
    scores = jnp.einsum(
        "nqhgd,nkhd->nhgqk", query_blocks, key_blocks, preferred_element_type=jnp.float32
    ) * HD ** (-0.5)
    scores = jnp.where(visible[:, None, None], scores, NEG_FILL)
    sink_col = sink_logits.reshape(kv_local, grouping)[None, :, :, None]
    top = jnp.maximum(jnp.max(scores, axis=-1), sink_col)
    expo = jnp.exp(scores - top[..., None])
    total = jnp.sum(expo, axis=-1) + jnp.exp(sink_col - top)
    probs = (expo / total[..., None]).astype(jnp.bfloat16)
    result = jnp.einsum(
        "nhgqk,nkhd->nqhgd", probs, value_blocks, preferred_element_type=jnp.float32
    )
    return result.astype(jnp.bfloat16).reshape(length, queries.shape[1])


def causal_local(upward, earlier, kernel):
    length = upward.shape[0]
    padded = jnp.concatenate([earlier, upward], axis=0).astype(jnp.float32)
    result = jnp.zeros(upward.shape, jnp.float32)
    for tap_index in range(kernel.shape[0]):
        result = result + kernel[tap_index][None, :] * padded[tap_index : tap_index + length]
    return result


def on_device(
    queries,
    key_states,
    value_states,
    sink_logits,
    out_weight,
    residual,
    gain_attn,
    gain_before,
    gain_after,
    gate_weight,
    value_weight,
    gate_taps,
    value_taps,
    down_weight,
):
    length = queries.shape[0]
    attended = attention_local(queries, key_states, value_states, sink_logits)
    selected = attended
    attn_proj = sum_at_owner(
        jnp.dot(selected, out_weight, preferred_element_type=jnp.float32).astype(jnp.bfloat16),
        "tp",
        0,
    )
    middle = residual.astype(jnp.float32) + rms_scale(attn_proj) * gain_attn
    normed = (rms_scale(middle) * gain_before).astype(jnp.bfloat16)
    whole_rows = gather_directly(normed, "tp", 0)
    gate_full, value_full = in_one_piece((gate_weight, value_weight), "sp", 0, 1)
    gate_up = jnp.dot(whole_rows, gate_full, preferred_element_type=jnp.float32).astype(
        jnp.bfloat16
    )
    value_up = jnp.dot(whole_rows, value_full, preferred_element_type=jnp.float32).astype(
        jnp.bfloat16
    )
    reach = gate_taps.shape[0] - 1
    gate_before, value_before = passed_along(
        (gate_up[length - reach :], value_up[length - reach :]), "sp", 1
    )
    gate_conv = causal_local(gate_up, gate_before, gate_taps)
    value_conv = causal_local(value_up, value_before, value_taps)
    hidden = (jax.nn.silu(gate_conv) * value_conv).astype(jnp.bfloat16)
    down_whole = lax.all_gather(down_weight, "sp", axis=1, tiled=True)
    selected = hidden
    down = sum_at_owner(
        jnp.dot(selected, down_whole, preferred_element_type=jnp.float32).astype(jnp.bfloat16),
        "tp",
        0,
    )
    return (middle + rms_scale(down) * gain_after).astype(jnp.bfloat16)


def solution(mesh):
    in_specs = (
        P("sp", "tp"),
        P("sp", "tp"),
        P("sp", "tp"),
        P("tp"),
        P("tp", None),
        P(("sp", "tp"), None),
        P(),
        P(),
        P(),
        P("sp", "tp"),
        P("sp", "tp"),
        P(None, "tp"),
        P(None, "tp"),
        P("tp", "sp"),
    )
    out_specs = P(("sp", "tp"), None)
    return jax.shard_map(
        on_device, mesh=mesh, in_specs=in_specs, out_specs=out_specs, check_vma=False
    )
```

profile of v0, /device:TPU:1, one launch (start us, length us, event | category | flops | bytes accessed | tf_op | source)
XLA Modules:
  0.0 238.2 jit_solution(13050096968348563992)
XLA Ops:
  6.5 1.6 pad_maximum_fusion
  8.2 0.7 slice.72
  8.9 4.0 %collective-permute-start.1 = (bf16[128,64]{0,1:T(8,128)(2,1)S(1)}, bf16[128,64]{0,1:T(8,128)(2,1)S(1)}, u32[]{:S(2)}, u32[]{:S(2)}) collective-permute-start(bf16[128,64]{0,1:T(8,128)(2,1)S(1)} %slice.72), channel_id=1, source_target_pairs={{0,8},{8,16},{16,24},{24,32},{32,40},{40,48},{48,56},{56,64},{64,7... | collective-permute-start | bytes 49160 | tf_op jit(solution)/shard_map/ppermute | solution.py:14
  13.0 0.7 slice.68
  13.7 3.2 %collective-permute-start = (bf16[128,64]{0,1:T(8,128)(2,1)S(1)}, bf16[128,64]{0,1:T(8,128)(2,1)S(1)}, u32[]{:S(2)}, u32[]{:S(2)}) collective-permute-start(bf16[128,64]{0,1:T(8,128)(2,1)S(1)} %slice.68), channel_id=1, source_target_pairs={{0,8},{8,16},{16,24},{24,32},{32,40},{40,48},{48,56},{56,64},{64,7... | collective-permute-start | bytes 49160 | tf_op jit(solution)/shard_map/ppermute | solution.py:14
  17.3 0.9 slice.75
  18.1 0.9 slice.71
  19.0 1.2 reshape.136
  20.3 0.8 pad_maximum_fusion.1
  21.2 0.5 fusion.39
  22.3 0.5 fusion.17
  23.0 2.1 convolution_convert_fusion
  25.1 6.4 %all-to-all-start = ((bf16[8,64,2048]{2,1,0:T(8,128)(2,1)}), bf16[8,64,2048]{2,1,0:T(8,128)(2,1)}, u32[]{:S(2)}, u32[]{:S(2)}) async-start(bf16[8,64,2048]{2,1,0:T(8,128)(2,1)} %bitcast.11), calls=%async_computation | async-start | bytes 4194304 | tf_op jit(solution)/shard_map/all_to_all | solution.py:24
  31.6 0.7 all-gather.5.cloned.1.call-update
  32.3 25.6 %all-to-all-done = bf16[8,64,2048]{2,1,0:T(8,128)(2,1)} async-done(((bf16[8,64,2048]{2,1,0:T(8,128)(2,1)}), bf16[8,64,2048]{2,1,0:T(8,128)(2,1)}, u32[]{:S(2)}, u32[]{:S(2)}) %all-to-all-start) | async-done | bytes 2097184 | tf_op jit(solution)/shard_map/all_to_all | solution.py:24
  57.9 2.0 convert_reduce_fusion.1
  60.5 1.6 broadcast_in_dim.16
  62.1 5.3 %all-to-all-start.1 = ((bf16[8,64,2048]{2,1,0:T(8,128)(2,1)}), bf16[8,64,2048]{2,1,0:T(8,128)(2,1)}, u32[]{:S(2)}, u32[]{:S(2)}) async-start(bf16[8,64,2048]{2,1,0:T(8,128)(2,1)} %broadcast_in_dim.16), calls=%async_computation.1 | async-start | bytes 4194304 | tf_op jit(solution)/shard_map/all_to_all | solution.py:36
  67.6 26.3 %all-to-all-done.1 = bf16[8,64,2048]{2,1,0:T(8,128)(2,1)} async-done(((bf16[8,64,2048]{2,1,0:T(8,128)(2,1)}), bf16[8,64,2048]{2,1,0:T(8,128)(2,1)}, u32[]{:S(2)}, u32[]{:S(2)}) %all-to-all-start.1) | async-done | bytes 2097184 | tf_op jit(solution)/shard_map/all_to_all | solution.py:36
  93.8 8.4 %all-gather.3.cloned.1.call-done = bf16[2048,1408]{1,0:T(8,128)(2,1)} async-done(((bf16[32,1408]{1,0:T(8,128)(2,1)}), bf16[2048,1408]{1,0:T(8,128)(2,1)}) %all-gather.3.cloned.1.call-update) | async-done | bytes 5767184 | tf_op jit(solution)/shard_map/all_gather | solution.py:46
  102.2 4.4 %fusion.11 = bf16[512,704]{0,1:T(8,128)(2,1)S(1)} fusion(bf16[512,2048]{1,0:T(8,128)(2,1)} %bitcast.12, bf16[2048,1408]{1,0:T(8,128)(2,1)} %all-gather.3.cloned.1.call-done), kind=kOutput, calls=%fused_computation.24 | convolution fusion | flops 1476755456 | bytes 5963776 | tf_op jit(solution)/shard_map/dot_general | solution.py:131
  106.7 2.7 %collective-permute-start.2 = (bf16[2,704]{0,1:T(8,128)(2,1)S(1)}, bf16[2,704]{0,1:T(8,128)(2,1)S(1)}, u32[]{:S(2)}, u32[]{:S(2)}) collective-permute-start(bf16[2,704]{0,1:T(8,128)(2,1)S(1)} %slice.90), channel_id=1, source_target_pairs={{0,8},{8,16},{16,24},{24,32},{32,40},{40,48},{48,56},{56,64},{64,7... | collective-permute-start | bytes 8456 | tf_op jit(solution)/shard_map/ppermute | solution.py:14
  109.4 4.5 %fusion.14 = bf16[512,704]{0,1:T(8,128)(2,1)S(1)} fusion(bf16[512,2048]{1,0:T(8,128)(2,1)} %bitcast.12, bf16[2048,1408]{1,0:T(8,128)(2,1)S(1)} %copy-done.9), kind=kOutput, calls=%fused_computation.25 | convolution fusion | flops 1476755456 | bytes 5963776 | tf_op jit(solution)/shard_map/dot_general | solution.py:134
  114.0 3.7 %collective-permute-start.3 = (bf16[2,704]{0,1:T(8,128)(2,1)S(1)}, bf16[2,704]{0,1:T(8,128)(2,1)S(1)}, u32[]{:S(2)}, u32[]{:S(2)}) collective-permute-start(bf16[2,704]{0,1:T(8,128)(2,1)S(1)} %slice.94), channel_id=1, source_target_pairs={{0,8},{8,16},{16,24},{24,32},{32,40},{40,48},{48,56},{56,64},{64,7... | collective-permute-start | bytes 8456 | tf_op jit(solution)/shard_map/ppermute | solution.py:14
  117.7 1.6 maximum_convert_fusion
  119.3 0.6 collective-permute-done.3
  119.9 1.6 maximum_convert_fusion.1
  121.5 64.6 %all-gather.5.cloned.1.call-done = bf16[704,2048]{0,1:T(8,128)(2,1)} async-done(((bf16[704,32]{0,1:T(8,128)(2,1)}), bf16[704,2048]{0,1:T(8,128)(2,1)}) %all-gather.5.cloned.1.call-update) | async-done | bytes 2883600 | tf_op jit(solution)/shard_map/all_gather | solution.py:144
  186.1 9.1 %convolution_convert_fusion.1 = bf16[512,2048]{1,0:T(8,128)(2,1)S(1)} fusion(bf16[704,2048]{0,1:T(8,128)(2,1)} %all-gather.5.cloned.1.call-done, f32[514,704]{0,1:T(8,128)} %maximum_convert_fusion.1, f32[514,704]{0,1:T(8,128)} %maximum_convert_fusion, f32[704]{0:T(1024)S(1)} %get-tuple-element.9, f32[704]{0:T(1024)S(1)} %get-tuple-element.10, ...), kind=kOutput, calls=%fused_computation.7 | convolution fusion | flops 1483210752 | bytes 13910528 | tf_op jit(solution)/shard_map/dot_general | solution.py:147
  195.2 34.6 %all_to_all.15 = bf16[8,64,2048]{2,1,0:T(8,128)(2,1)S(1)} all-to-all(bf16[8,64,2048]{2,1,0:T(8,128)(2,1)S(1)} %bitcast.47), channel_id=1, replica_groups=mesh['sp'=64,'tp'=8] {'tp'}, dimensions={0} | all-to-all | bytes 4194304 | tf_op jit(solution)/shard_map/all_to_all | solution.py:24
  229.8 0.4 convert_reduce_fusion
  230.5 0.9 add_convert_fusion
  (52 shorter events, 2.5 us)
Async XLA Ops:
  6.5 16.4 %copy-start = (bf16[256,2048]{1,0:T(8,128)(2,1)S(1)}, bf16[256,2048]{1,0:T(8,128)(2,1)}, u32[]{:S(2)}) copy-start(bf16[256,2048]{1,0:T(8,128)(2,1)} %param.18) | copy-start | bytes 3145732
  6.5 14.6 %copy-start.2 = (bf16[512,64]{0,1:T(8,128)(2,1)S(1)}, bf16[512,64]{0,1:T(8,128)(2,1)}, u32[]{:S(2)}) copy-start(bf16[512,64]{0,1:T(8,128)(2,1)} %param.16) | copy-start | bytes 196612
  6.5 95.7 %all-gather.3.cloned.1.call-start = ((), (), s32[]{:S(2)}) async-start(), calls=%async_computation.3 | async-start | bytes 5857280 | tf_op jit(solution)/shard_map/all_gather | solution.py:46
  8.9 11.4 %collective-permute-start.1 = (bf16[128,64]{0,1:T(8,128)(2,1)S(1)}, bf16[128,64]{0,1:T(8,128)(2,1)S(1)}, u32[]{:S(2)}, u32[]{:S(2)}) collective-permute-start(bf16[128,64]{0,1:T(8,128)(2,1)S(1)} %slice.72), channel_id=1, source_target_pairs={{0,8},{8,16},{16,24},{24,32},{32,40},{40,48},{48,56},{56,64},{64,7... | collective-permute-start | bytes 49160 | tf_op jit(solution)/shard_map/ppermute | solution.py:14
  13.7 7.5 %collective-permute-start = (bf16[128,64]{0,1:T(8,128)(2,1)S(1)}, bf16[128,64]{0,1:T(8,128)(2,1)S(1)}, u32[]{:S(2)}, u32[]{:S(2)}) collective-permute-start(bf16[128,64]{0,1:T(8,128)(2,1)S(1)} %slice.68), channel_id=1, source_target_pairs={{0,8},{8,16},{16,24},{24,32},{32,40},{40,48},{48,56},{56,64},{64,7... | collective-permute-start | bytes 49160 | tf_op jit(solution)/shard_map/ppermute | solution.py:14
  20.2 1.5 copy-start.8
  25.1 32.8 %all-to-all-start = ((bf16[8,64,2048]{2,1,0:T(8,128)(2,1)}), bf16[8,64,2048]{2,1,0:T(8,128)(2,1)}, u32[]{:S(2)}, u32[]{:S(2)}) async-start(bf16[8,64,2048]{2,1,0:T(8,128)(2,1)} %bitcast.11), calls=%async_computation | async-start | bytes 4194304 | tf_op jit(solution)/shard_map/all_to_all | solution.py:24
  31.5 28.5 %copy-start.1 = (bf16[64,2048]{1,0:T(8,128)(2,1)S(1)}, bf16[64,2048]{1,0:T(8,128)(2,1)}, u32[]{:S(2)}) copy-start(bf16[64,2048]{1,0:T(8,128)(2,1)} %param.19) | copy-start | bytes 786436
  31.5 28.5 %copy-start.3 = (f32[2048]{0:T(1024)S(1)}, f32[2048]{0:T(1024)}, u32[]{:S(2)}) copy-start(f32[2048]{0:T(1024)} %param.20) | copy-start | bytes 24580
  31.5 28.8 %copy-start.4 = (f32[2048]{0:T(1024)S(1)}, f32[2048]{0:T(1024)}, u32[]{:S(2)}) copy-start(f32[2048]{0:T(1024)} %param.21) | copy-start | bytes 24580
  31.5 154.6 %all-gather.5.cloned.1.call-start = ((), (), s32[]{:S(2)}) async-start(), calls=%async_computation.4 | async-start | bytes 3194880 | tf_op jit(solution)/shard_map/all_gather | solution.py:144
  62.1 5.3 %copy-start.6 = (f32[3,704]{1,0:T(4,128)S(1)}, f32[3,704]{1,0:T(4,128)}, u32[]{:S(2)}) copy-start(f32[3,704]{1,0:T(4,128)} %param.26) | copy-start | bytes 25348
  62.1 5.3 %copy-start.7 = (f32[3,704]{1,0:T(4,128)S(1)}, f32[3,704]{1,0:T(4,128)}, u32[]{:S(2)}) copy-start(f32[3,704]{1,0:T(4,128)} %param.25) | copy-start | bytes 25348
  62.1 31.7 %all-to-all-start.1 = ((bf16[8,64,2048]{2,1,0:T(8,128)(2,1)}), bf16[8,64,2048]{2,1,0:T(8,128)(2,1)}, u32[]{:S(2)}, u32[]{:S(2)}) async-start(bf16[8,64,2048]{2,1,0:T(8,128)(2,1)} %broadcast_in_dim.16), calls=%async_computation.1 | async-start | bytes 4194304 | tf_op jit(solution)/shard_map/all_to_all | solution.py:36
  102.2 7.2 %copy-start.9 = (bf16[2048,1408]{1,0:T(8,128)(2,1)S(1)}, bf16[2048,1408]{1,0:T(8,128)(2,1)}, u32[]{:S(2)}) copy-start(bf16[2048,1408]{1,0:T(8,128)(2,1)} %all-gather.3.cloned.1.call-done) | copy-start | bytes 17301508
  106.7 11.0 %collective-permute-start.2 = (bf16[2,704]{0,1:T(8,128)(2,1)S(1)}, bf16[2,704]{0,1:T(8,128)(2,1)S(1)}, u32[]{:S(2)}, u32[]{:S(2)}) collective-permute-start(bf16[2,704]{0,1:T(8,128)(2,1)S(1)} %slice.90), channel_id=1, source_target_pairs={{0,8},{8,16},{16,24},{24,32},{32,40},{40,48},{48,56},{56,64},{64,7... | collective-permute-start | bytes 8456 | tf_op jit(solution)/shard_map/ppermute | solution.py:14
  114.0 5.9 %collective-permute-start.3 = (bf16[2,704]{0,1:T(8,128)(2,1)S(1)}, bf16[2,704]{0,1:T(8,128)(2,1)S(1)}, u32[]{:S(2)}, u32[]{:S(2)}) collective-permute-start(bf16[2,704]{0,1:T(8,128)(2,1)S(1)} %slice.94), channel_id=1, source_target_pairs={{0,8},{8,16},{16,24},{24,32},{32,40},{40,48},{48,56},{56,64},{64,7... | collective-permute-start | bytes 8456 | tf_op jit(solution)/shard_map/ppermute | solution.py:14
  229.8 0.7 copy-start.5
Sparse Core Ops, SparseCore 0:
  10.3 91.8 all-gather.2
  105.2 80.8 all-gather.4
where the time goes:
time: 239 us; the launch traced here: 238 us
  waiting for transfers between devices  126 us (53%)
  blocking collectives  34.6 us (14%)
  starting transfers between devices  25.4 us (11%)
  matrix products  21 us (9%)
  between operations  13.7 us (6%)
  other arithmetic  10.6 us (4%)
  local copies, waits for them, and re-layouts  6.82 us (3%)
    all_gather x1, waiting for transfers between devices, on_device(): down_whole = lax.all_gather(down_weight, 'sp', axis=1, tiled=True)  64.6 us
    all_to_all x1, blocking collectives, sum_at_owner(): lax.all_to_all(in_blocks(shard, dim, peers), axis, 0, 0, tiled=True)  34.6 us
    all_to_all x1, waiting for transfers between devices, sent_to_all(): return lax.all_to_all(copies, axis, split_axis=0, concat_axis=0, tiled=True)  26.3 us
    all_to_all x1, waiting for transfers between devices, sum_at_owner(): lax.all_to_all(in_blocks(shard, dim, peers), axis, 0, 0, tiled=True)  25.6 us
    ppermute x4, starting transfers between devices, passed_along(): return lax.ppermute(block, axis, route)  13.5 us
    dot_general x1, matrix products, on_device(): jnp.dot(selected, down_whole, preferred_element_type=jnp.float32)  9.1 us
    all_gather x1, waiting for transfers between devices, in_one_piece(): filled = lax.all_gather(both, axis, axis=dim, tiled=True)  8.4 us
    all_to_all x1, starting transfers between devices, sum_at_owner(): lax.all_to_all(in_blocks(shard, dim, peers), axis, 0, 0, tiled=True)  6.45 us
  transfers between devices with their start and end apart: 8, of which 5 were waited for; matrix products, arithmetic and copies ran while one was open for 11% of the time, Pallas kernels for 0%

commit v1 on v0

--- a/solution.py
+++ b/solution.py
@@ -141,7 +141,11 @@
     gate_conv = causal_local(gate_up, gate_before, gate_taps)
     value_conv = causal_local(value_up, value_before, value_taps)
     hidden = (jax.nn.silu(gate_conv) * value_conv).astype(jnp.bfloat16)
-    down_whole = lax.all_gather(down_weight, "sp", axis=1, tiled=True)
+    size = lax.axis_size("sp")
+    repeats = [size if d == 1 else 1 for d in range(down_weight.ndim)]
+    down_whole = lax.all_to_all(
+        jnp.tile(down_weight, repeats), "sp", split_axis=1, concat_axis=1, tiled=True
+    )
     selected = hidden
     down = sum_at_owner(
         jnp.dot(selected, down_whole, preferred_element_type=jnp.float32).astype(jnp.bfloat16),

time: 239 us -> 246 us (1.029)
  the two profiles are of different devices: /device:TPU:1 before, /device:TPU:80 now
where the time goes in v1:
time: 246 us; the launch traced here: 245 us
  blocking collectives  108 us (44%)
  waiting for transfers between devices  63.6 us (26%)
  starting transfers between devices  25 us (10%)
  matrix products  18.1 us (7%)
  between operations  13.7 us (6%)
  other arithmetic  8.84 us (4%)
  local copies, waits for them, and re-layouts  8.03 us (3%)
    all_to_all x2, blocking collectives, sum_at_owner(): lax.all_to_all(in_blocks(shard, dim, peers), axis, 0, 0, tiled=True)  77.5 us
    all_gather x1, waiting for transfers between devices, in_one_piece(): filled = lax.all_gather(both, axis, axis=dim, tiled=True)  33.5 us
    all_to_all x1, blocking collectives, sent_to_all(): return lax.all_to_all(copies, axis, split_axis=0, concat_axis=0, tiled=True)  30.5 us
    ppermute x4, waiting for transfers between devices, passed_along(): return lax.ppermute(block, axis, route)  30.1 us
    all_to_all x1, starting transfers between devices, on_device(): lax.all_to_all(jnp.tile(down_weight, repeats), 'sp', split_axis=1, concat...  12.8 us
    ppermute x4, starting transfers between devices, passed_along(): return lax.ppermute(block, axis, route)  12.2 us
    dot_general x1, matrix products, on_device(): jnp.dot(selected, down_whole, preferred_element_type=jnp.float32)  9.12 us
  transfers between devices with their start and end apart: 6, of which 3 were waited for; matrix products, arithmetic and copies ran while one was open for 9% of the time, Pallas kernels for 0%

profile of v1, /device:TPU:80, one launch (start us, length us, event | category | flops | bytes accessed | tf_op | source)
XLA Modules:
  0.0 245.4 jit_solution(11304663870542470977)
XLA Ops:
  6.5 0.8 slice.68
  7.4 3.5 %collective-permute-start = (bf16[128,64]{0,1:T(8,128)(2,1)S(1)}, bf16[128,64]{0,1:T(8,128)(2,1)S(1)}, u32[]{:S(2)}, u32[]{:S(2)}) collective-permute-start(bf16[128,64]{0,1:T(8,128)(2,1)S(1)} %slice.68), channel_id=1, source_target_pairs={{0,8},{8,16},{16,24},{24,32},{32,40},{40,48},{48,56},{56,64},{64,7... | collective-permute-start | bytes 49160 | tf_op jit(solution)/shard_map/ppermute | solution.py:14
  10.8 0.7 slice.72
  11.6 4.7 %collective-permute-start.1 = (bf16[128,64]{0,1:T(8,128)(2,1)S(1)}, bf16[128,64]{0,1:T(8,128)(2,1)S(1)}, u32[]{:S(2)}, u32[]{:S(2)}) collective-permute-start(bf16[128,64]{0,1:T(8,128)(2,1)S(1)} %slice.72), channel_id=1, source_target_pairs={{0,8},{8,16},{16,24},{24,32},{32,40},{40,48},{48,56},{56,64},{64,7... | collective-permute-start | bytes 49160 | tf_op jit(solution)/shard_map/ppermute | solution.py:14
  16.3 1.5 pad_maximum_fusion
  17.9 0.3 fusion.29
  18.2 0.9 slice.75
  19.1 0.9 slice.71
  20.0 1.2 reshape.143
  21.3 0.8 pad_maximum_fusion.1
  22.2 0.5 fusion.39
  23.2 0.5 fusion.17
  23.9 0.7 convolution_convert_fusion
  24.7 31.3 %all_to_all.24 = bf16[8,64,2048]{2,1,0:T(8,128)(2,1)S(1)} all-to-all(bf16[8,64,2048]{2,1,0:T(8,128)(2,1)S(1)} %bitcast.48), channel_id=1, replica_groups=mesh['sp'=64,'tp'=8] {'tp'}, dimensions={0} | all-to-all | bytes 4194304 | tf_op jit(solution)/shard_map/all_to_all | solution.py:24
  56.0 0.4 convert_reduce_fusion.1
  56.5 0.4 copy-done.1
  57.7 30.5 %all_to_all.25 = bf16[8,64,2048]{2,1,0:T(8,128)(2,1)} all-to-all(bf16[8,64,2048]{2,1,0:T(8,128)(2,1)S(1)} %broadcast_in_dim.16), channel_id=1, replica_groups=mesh['sp'=64,'tp'=8] {'tp'}, dimensions={0} | all-to-all | bytes 4194304 | tf_op jit(solution)/shard_map/all_to_all | solution.py:36
  88.2 2.0 tile.2
  90.3 12.8 %all-to-all-start.2 = ((bf16[704,64,32]{0,2,1:T(8,128)(2,1)}), bf16[704,64,32]{0,2,1:T(8,128)(2,1)}, u32[]{:S(2)}, u32[]{:S(2)}) async-start(bf16[704,64,32]{0,2,1:T(8,128)(2,1)} %tile.2), calls=%async_computation.2 | async-start | bytes 6291456 | tf_op jit(solution)/shard_map/all_to_all | solution.py:146
  103.2 33.5 %all-gather.2.cloned.1.call-done = bf16[2048,1408]{1,0:T(8,128)(2,1)} async-done(((bf16[32,1408]{1,0:T(8,128)(2,1)}), bf16[2048,1408]{1,0:T(8,128)(2,1)}) %all-gather.2.cloned.1.call-update) | async-done | bytes 5767184 | tf_op jit(solution)/shard_map/all_gather | solution.py:46
  136.7 4.4 %fusion.11 = bf16[512,704]{0,1:T(8,128)(2,1)S(1)} fusion(bf16[512,2048]{1,0:T(8,128)(2,1)} %bitcast.49, bf16[2048,1408]{1,0:T(8,128)(2,1)} %all-gather.2.cloned.1.call-done), kind=kOutput, calls=%fused_computation.24 | convolution fusion | flops 1476755456 | bytes 5963776 | tf_op jit(solution)/shard_map/dot_general | solution.py:131
  141.2 1.9 collective-permute-start.2
  143.1 2.9 %fusion.14 = bf16[512,704]{0,1:T(8,128)(2,1)S(1)} fusion(bf16[512,2048]{1,0:T(8,128)(2,1)S(1)} %bitcast.50, bf16[2048,1408]{1,0:T(8,128)(2,1)S(1)} %copy-done.11), kind=kOutput, calls=%fused_computation.25 | convolution fusion | flops 1476755456 | bytes 5963776 | tf_op jit(solution)/shard_map/dot_general | solution.py:134
  146.1 2.1 collective-permute-start.3
  148.2 28.3 %collective-permute-done.2 = bf16[2,704]{0,1:T(8,128)(2,1)S(1)} collective-permute-done((bf16[2,704]{0,1:T(8,128)(2,1)S(1)}, bf16[2,704]{0,1:T(8,128)(2,1)S(1)}, u32[]{:S(2)}, u32[]{:S(2)}) %collective-permute-start.2) | collective-permute-done | bytes 2848 | tf_op jit(solution)/shard_map/ppermute | solution.py:14
  176.6 1.6 maximum_convert_fusion
  178.2 1.8 collective-permute-done.3
  180.0 1.6 maximum_convert_fusion.1
  181.6 9.1 %convolution_convert_fusion.1 = bf16[512,2048]{1,0:T(8,128)(2,1)S(1)} fusion(bf16[704,2048]{0,1:T(8,128)(2,1)} %bitcast.13, f32[514,704]{0,1:T(8,128)} %maximum_convert_fusion.1, f32[514,704]{0,1:T(8,128)} %maximum_convert_fusion, f32[704]{0:T(1024)S(1)} %get-tuple-element.9, f32[704]{0:T(1024)S(1)} %get-tuple-element.10, f32[704]{0:T(1024)S(1)} %get-tuple-element.8, ...), kind=kOutput, calls=%fused_computation.7 | convolution fusion | flops 1483210752 | bytes 13910528 | tf_op jit(solution)/shard_map/dot_general | solution.py:151
  190.7 46.2 %all_to_all.26 = bf16[8,64,2048]{2,1,0:T(8,128)(2,1)S(1)} all-to-all(bf16[8,64,2048]{2,1,0:T(8,128)(2,1)S(1)} %bitcast.51), channel_id=1, replica_groups=mesh['sp'=64,'tp'=8] {'tp'}, dimensions={0} | all-to-all | bytes 4194304 | tf_op jit(solution)/shard_map/all_to_all | solution.py:24
  236.9 0.4 convert_reduce_fusion
  237.6 0.9 add_convert_fusion
  (54 shorter events, 2.3 us)
Async XLA Ops:
  6.5 17.4 %copy-start = (bf16[256,2048]{1,0:T(8,128)(2,1)S(1)}, bf16[256,2048]{1,0:T(8,128)(2,1)}, u32[]{:S(2)}) copy-start(bf16[256,2048]{1,0:T(8,128)(2,1)} %param.18) | copy-start | bytes 3145732
  6.5 15.6 %copy-start.3 = (bf16[512,64]{0,1:T(8,128)(2,1)S(1)}, bf16[512,64]{0,1:T(8,128)(2,1)}, u32[]{:S(2)}) copy-start(bf16[512,64]{0,1:T(8,128)(2,1)} %param.16) | copy-start | bytes 196612
  6.5 130.1 %all-gather.2.cloned.1.call-start = ((), (), s32[]{:S(2)}) async-start(), calls=%async_computation.4 | async-start | bytes 5857280 | tf_op jit(solution)/shard_map/all_gather | solution.py:46
  7.4 14.8 %collective-permute-start = (bf16[128,64]{0,1:T(8,128)(2,1)S(1)}, bf16[128,64]{0,1:T(8,128)(2,1)S(1)}, u32[]{:S(2)}, u32[]{:S(2)}) collective-permute-start(bf16[128,64]{0,1:T(8,128)(2,1)S(1)} %slice.68), channel_id=1, source_target_pairs={{0,8},{8,16},{16,24},{24,32},{32,40},{40,48},{48,56},{56,64},{64,7... | collective-permute-start | bytes 49160 | tf_op jit(solution)/shard_map/ppermute | solution.py:14
  11.6 9.7 %collective-permute-start.1 = (bf16[128,64]{0,1:T(8,128)(2,1)S(1)}, bf16[128,64]{0,1:T(8,128)(2,1)S(1)}, u32[]{:S(2)}, u32[]{:S(2)}) collective-permute-start(bf16[128,64]{0,1:T(8,128)(2,1)S(1)} %slice.72), channel_id=1, source_target_pairs={{0,8},{8,16},{16,24},{24,32},{32,40},{40,48},{48,56},{56,64},{64,7... | collective-permute-start | bytes 49160 | tf_op jit(solution)/shard_map/ppermute | solution.py:14
  20.0 2.7 %copy-start.10 = (f32[4]{0:T(128)S(1)}, f32[4]{0:T(128)}, u32[]{:S(2)}) copy-start(f32[4]{0:T(128)} %param.17) | copy-start | bytes 52
  56.0 1.0 copy-start.1
  56.0 1.0 copy-start.4
  56.0 1.2 copy-start.6
  57.7 30.5 %copy-start.5 = (bf16[704,32]{0,1:T(8,128)(2,1)S(1)}, bf16[704,32]{0,1:T(8,128)(2,1)}, u32[]{:S(2)}) copy-start(bf16[704,32]{0,1:T(8,128)(2,1)} %param.27) | copy-start | bytes 135172
  90.3 12.9 %copy-start.8 = (f32[3,704]{1,0:T(4,128)S(1)}, f32[3,704]{1,0:T(4,128)}, u32[]{:S(2)}) copy-start(f32[3,704]{1,0:T(4,128)} %param.26) | copy-start | bytes 25348
  90.3 12.9 %copy-start.9 = (f32[3,704]{1,0:T(4,128)S(1)}, f32[3,704]{1,0:T(4,128)}, u32[]{:S(2)}) copy-start(f32[3,704]{1,0:T(4,128)} %param.25) | copy-start | bytes 25348
  90.3 91.3 %all-to-all-start.2 = ((bf16[704,64,32]{0,2,1:T(8,128)(2,1)}), bf16[704,64,32]{0,2,1:T(8,128)(2,1)}, u32[]{:S(2)}, u32[]{:S(2)}) async-start(bf16[704,64,32]{0,2,1:T(8,128)(2,1)} %tile.2), calls=%async_computation.2 | async-start | bytes 6291456 | tf_op jit(solution)/shard_map/all_to_all | solution.py:146
  136.7 6.4 %copy-start.2 = (bf16[8,64,2048]{2,1,0:T(8,128)(2,1)S(1)}, bf16[8,64,2048]{2,1,0:T(8,128)(2,1)}, u32[]{:S(2)}) copy-start(bf16[8,64,2048]{2,1,0:T(8,128)(2,1)} %all_to_all.25) | copy-start | bytes 6291460
  136.7 6.4 %copy-start.11 = (bf16[2048,1408]{1,0:T(8,128)(2,1)S(1)}, bf16[2048,1408]{1,0:T(8,128)(2,1)}, u32[]{:S(2)}) copy-start(bf16[2048,1408]{1,0:T(8,128)(2,1)} %all-gather.2.cloned.1.call-done) | copy-start | bytes 17301508
  141.2 35.4 %collective-permute-start.2 = (bf16[2,704]{0,1:T(8,128)(2,1)S(1)}, bf16[2,704]{0,1:T(8,128)(2,1)S(1)}, u32[]{:S(2)}, u32[]{:S(2)}) collective-permute-start(bf16[2,704]{0,1:T(8,128)(2,1)S(1)} %slice.90), channel_id=1, source_target_pairs={{0,8},{8,16},{16,24},{24,32},{32,40},{40,48},{48,56},{56,64},{64,7... | collective-permute-start | bytes 8456 | tf_op jit(solution)/shard_map/ppermute | solution.py:14
  146.1 33.8 %collective-permute-start.3 = (bf16[2,704]{0,1:T(8,128)(2,1)S(1)}, bf16[2,704]{0,1:T(8,128)(2,1)S(1)}, u32[]{:S(2)}, u32[]{:S(2)}) collective-permute-start(bf16[2,704]{0,1:T(8,128)(2,1)S(1)} %slice.94), channel_id=1, source_target_pairs={{0,8},{8,16},{16,24},{24,32},{32,40},{40,48},{48,56},{56,64},{64,7... | collective-permute-start | bytes 8456 | tf_op jit(solution)/shard_map/ppermute | solution.py:14
  236.9 0.7 copy-start.7
Sparse Core Ops, SparseCore 0:
  17.9 118.6 all-gather.1
